TPU v7x, 32 devices: a whole 2x2x4 slice. The times are simulated.
32 devices in a mesh: grp: 2 (over y), sp: 4 (over z), tp: 4 (over x, core).
Axes of the slice: x: 2, y: 2, z: 4, core: 2. Of those that a mesh axis runs over, the one named last changes fastest.
Arguments:
- query_rows: bfloat16 [1024, 1024], P(('grp', 'sp'), 'tp'), parts along dimension 0, may hold values from -12 to 12
- key_rows: bfloat16 [1024, 1024], P(('grp', 'sp'), 'tp'), parts along dimension 0, may hold values from -9 to 9
- value_rows: bfloat16 [1024, 1024], P(('grp', 'sp'), 'tp'), parts along dimension 0, may hold values from -6 to 6
- key_logit: bfloat16 [1024, 8], P(('grp', 'sp'), 'tp'), parts along dimension 0, as said below
- residual: bfloat16 [1024, 2048], P(('grp', 'sp')), parts along dimension 0, may hold values from -6 to 6
- out_weight: bfloat16 [1024, 2048], P('tp'), may hold values from -0.1875 to 0.1875
- mix_gain: float32 [2048], replicated, may hold values from 0.1 to 1.9
- ffn_gain: float32 [2048], replicated, may hold values from 0.1 to 1.9
- out_gain: float32 [2048], replicated, may hold values from 0.1 to 1.9
- gate_weight: bfloat16 [2048, 5120], P('sp', 'tp'), may hold values from -0.125 to 0.125
- up_weight: bfloat16 [2048, 5120], P('sp', 'tp'), may hold values from -0.125 to 0.125
- down_weight: bfloat16 [2048, 5120], P('sp', 'tp'), may hold values from -0.078125 to 0.078125
Outputs:
- layer_out: bfloat16 [1024, 2048], P(('grp', 'sp')), parts along dimension 0
There are 2 independent parts, one for each index of `grp`. A program takes and returns all parts, laid end to end along the dimension named above; an argument that names none is the same for every part. Nothing has to cross between parts.
Inputs may be any that keep to these rules, and one draw needn't show every extreme that they name: `key_logit`: log-odds offsets of the keys, all negative.
All inputs are finite; a program needn't handle non-finite values.
Results may differ from a plain program's by a relative error of at most 0.018.
Values may be sent and summed in bfloat16 or wider, within the bound.
No kernel may reach another device: no remote copies, remote signals or barrier semaphores. Data moves between devices by JAX's collectives and lax.ppermute only.
A program may use at most 64 MiB of HBM per device.

v0:
```python
import jax
import jax.numpy as jnp
from jax import lax
from jax.sharding import PartitionSpec as P

epsilon = 1e-06


def normalize(payload_table):
    return payload_table * lax.rsqrt(
        jnp.mean(payload_table * payload_table, axis=-1, keepdims=True) + epsilon
    )


def shards(
    query_rows,
    key_rows,
    value_rows,
    key_logit,
    residual,
    out_weight,
    mix_gain,
    ffn_gain,
    out_gain,
    gate_weight,
    up_weight,
    down_weight,
):
    tok_rows = query_rows.shape[0]
    head_count = key_logit.shape[1]
    head_width = query_rows.shape[1] // head_count
    block_count = lax.axis_size("sp")
    own_block = lax.axis_index("sp")
    queries = query_rows.reshape(tok_rows, head_count, head_width).transpose(1, 0, 2)
    score_scale = head_width ** (-0.5)
    query_pos = own_block * tok_rows + jnp.arange(tok_rows, dtype=jnp.int32)[:, None]

    def group_terms(key_part, value_part, logit_part, first_block):
        span_rows = key_part.shape[0]
        shard_count = span_rows // tok_rows

        def compute(unused):
            scores = (
                jnp.einsum(
                    "hqd,khd->hqk",
                    queries,
                    key_part.reshape(span_rows, head_count, head_width),
                    preferred_element_type=jnp.float32,
                )
                * score_scale
            )
            scores = scores + jnp.transpose(logit_part.astype(jnp.float32))[:, None, :]
            key_pos = first_block * tok_rows + jnp.arange(span_rows, dtype=jnp.int32)[None, :]
            causal = (key_pos < query_pos).reshape(tok_rows, shard_count, tok_rows)
            scores = scores.reshape(head_count, tok_rows, shard_count, tok_rows)
            keep_log = jnp.where(causal, jax.nn.log_sigmoid(-scores), 0.0)
            within = lax.cumsum(keep_log, axis=3, reverse=True) - keep_log
            sticks = jnp.where(causal, jnp.exp(jax.nn.log_sigmoid(scores) + within), 0.0).astype(
                jnp.bfloat16
            )
            partials = jnp.einsum(
                "hqgk,gkhd->ghqd",
                sticks,
                value_part.reshape(shard_count, tok_rows, head_count, head_width),
                preferred_element_type=jnp.float32,
            )
            return (jnp.sum(keep_log, axis=3), partials)

        def skipped(unused):
            return (
                jnp.zeros((head_count, tok_rows, shard_count), jnp.float32),
                jnp.zeros((shard_count, head_count, tok_rows, head_width), jnp.float32),
            )

        return lax.cond(first_block <= own_block, compute, skipped, 0)

    initial = (
        jnp.zeros((head_count, tok_rows, block_count), jnp.float32),
        jnp.zeros((block_count, head_count, tok_rows, head_width), jnp.float32),
    )
    tables = initial
    key_part = lax.all_gather(key_rows, "sp", axis=0, tiled=True)
    value_part = lax.all_gather(value_rows, "sp", axis=0, tiled=True)
    logit_part = lax.all_gather(key_logit, "sp", axis=0, tiled=True)
    shard_count = key_part.shape[0] // tok_rows
    group_size = 2
    span_rows = group_size * tok_rows

    def one_group(carried, group_index):
        offset = group_index * span_rows
        first_block = group_index * group_size
        totals, partials = group_terms(
            lax.dynamic_slice_in_dim(key_part, offset, span_rows, 0),
            lax.dynamic_slice_in_dim(value_part, offset, span_rows, 0),
            lax.dynamic_slice_in_dim(logit_part, offset, span_rows, 0),
            first_block,
        )
        carried = (
            lax.dynamic_update_slice(carried[0], totals, (0, 0, first_block)),
            lax.dynamic_update_slice(carried[1], partials, (first_block, 0, 0, 0)),
        )
        return (carried, None)

    tables, unused = lax.scan(
        one_group, tables, jnp.arange(shard_count // group_size, dtype=jnp.int32)
    )
    totals, partials = tables
    suffix = lax.cumsum(totals, axis=2, reverse=True) - totals
    attended = jnp.einsum(
        "hqb,bhqd->qhd", jnp.exp(suffix), partials, precision=lax.Precision.HIGHEST
    )
    attended = attended.reshape(tok_rows, head_count * head_width).astype(jnp.bfloat16)
    head_part = jnp.dot(attended, out_weight, preferred_element_type=jnp.float32)
    mixed_rows = lax.psum(head_part.astype(jnp.bfloat16), "tp")
    middle = (
        residual.astype(jnp.float32) + mix_gain * normalize(mixed_rows.astype(jnp.float32))
    ).astype(jnp.bfloat16)
    normed = (ffn_gain * normalize(middle.astype(jnp.float32))).astype(jnp.bfloat16)
    gate_act = jnp.dot(
        normed,
        lax.all_gather(gate_weight, "sp", axis=0, tiled=True),
        preferred_element_type=jnp.float32,
    )
    up_act = jnp.dot(
        normed,
        lax.all_gather(up_weight, "sp", axis=0, tiled=True),
        preferred_element_type=jnp.float32,
    )
    hidden = (jax.nn.silu(gate_act) * up_act).astype(jnp.bfloat16)
    unit_part = lax.dot_general(
        hidden,
        lax.all_gather(down_weight, "sp", axis=0, tiled=True),
        (((1,), (1,)), ((), ())),
        preferred_element_type=jnp.float32,
    )
    ffn_out = lax.psum(unit_part.astype(jnp.bfloat16), "tp")
    return (middle.astype(jnp.float32) + out_gain * normalize(ffn_out.astype(jnp.float32))).astype(
        jnp.bfloat16
    )


def solution(mesh):
    placed = (
        P(("grp", "sp"), "tp"),
        P(("grp", "sp"), "tp"),
        P(("grp", "sp"), "tp"),
        P(("grp", "sp"), "tp"),
        P(("grp", "sp"), None),
        P("tp", None),
        P(),
        P(),
        P(),
        P("sp", "tp"),
        P("sp", "tp"),
        P("sp", "tp"),
    )
    return jax.shard_map(
        shards, mesh=mesh, in_specs=placed, out_specs=P(("grp", "sp"), None), check_vma=False
    )
```

profile of v0, /device:TPU:0, one launch (start us, length us, event | category | flops | bytes accessed | tf_op | source)
XLA Modules:
  0.0 408.5 jit_solution(9131922966451456633)
XLA Ops:
  7.4 1.0 copy.41
  8.4 14.5 %all_gather.18 = bf16[512,256]{0,1:T(8,128)(2,1)S(1)} all-gather(bf16[128,256]{0,1:T(8,128)(2,1)S(1)} %copy.41), channel_id=1, replica_groups=mesh['grp'=2,'sp'=4,'tp'=4] {'sp'}, dimensions={0}, use_global_device_ids=true | all-gather | bytes 327680 | tf_op jit(solution)/shard_map/all_gather | solution.py:82
  22.9 14.6 %all_gather.20 = bf16[512,256]{1,0:T(8,128)(2,1)S(1)} all-gather(bf16[128,256]{1,0:T(8,128)(2,1)} %param.18), channel_id=1, replica_groups=mesh['grp'=2,'sp'=4,'tp'=4] {'sp'}, dimensions={0}, use_global_device_ids=true | all-gather | bytes 327680 | tf_op jit(solution)/shard_map/all_gather | solution.py:83
  37.5 0.9 copy.42
  38.4 0.1 copy.43
  38.6 10.0 %all_gather.19 = bf16[512,2]{0,1:T(2,128)(2,1)S(1)} all-gather(bf16[128,2]{0,1:T(2,128)(2,1)} %param.19), channel_id=1, replica_groups=mesh['grp'=2,'sp'=4,'tp'=4] {'sp'}, dimensions={0}, use_global_device_ids=true | all-gather | bytes 2560 | tf_op jit(solution)/shard_map/all_gather | solution.py:84
  48.6 0.1 broadcast_in_dim.28.clone
  48.7 8.5 %while.13 = (s32[]{:T(128)}, f32[2,128,4]{1,2,0:T(4,128)S(1)}, f32[4,2,128,128]{3,0,1,2:T(4,128)S(1)}, s32[2]{0:T(128)S(1)}, s32[]{:T(128)}, /*index=5*/bf16[512...) while((s32[]{:T(128)}, f32[2,128,4]{1,2,0:T(4,128)S(1)}, ...), condition=%wide.region_5.6_spmd.clone, body=%wide.region_0.5_spmd.clone.sunk | while | flops 43418504 | bytes 4373875 | solution.py:104
  48.7 0.6 dynamic_slice.39
  49.9 5.3 %conditional.3 = (f32[2,128,2]{1,2,0:T(2,128)S(1)}, f32[2,2,128,128]{3,2,1,0:T(8,128)S(1)}) conditional(s32[]{:T(128)} %convert_element_type.116, () %tuple.48, (s32[]{:T(128)}, s32[]{:T(128)}, s32[]{:T(128)}, bf16[512,256]{0,1:T(8,128)(2,1)S(1)}, bf16[2,128,128]{2,1,0:T(8,128)(2,1)S(1)}, /*index=5*/bf16[512,2]{0,1:T(2,128)(2,1)S(1)}, ...), branch_computations={%region_1.1_spmd, %region_2.4_spmd} | conditional | flops 43418500 | bytes 3844702 | solution.py:75
  50.6 0.2 fusion.2
  50.9 0.2 broadcast_compare_fusion
  51.1 0.8 fusion.35
  51.9 2.2 fusion.38
  54.0 0.9 select_convert_fusion
  55.0 0.2 fusion.8
  55.2 0.3 copy_dynamic-update-slice_fusion.2
  55.6 0.6 dynamic_slice.39
  56.9 0.3 copy_dynamic-update-slice_fusion.2
  57.2 0.0 copy-start.1
  57.2 0.0 copy-start.2
  57.2 0.0 copy-start.3
  57.3 0.2 copy.45
  57.5 1.8 fusion.39
  59.3 1.1 convolution_convert_fusion.1
  60.4 0.0 all-reduce.3.cloned.1.call-update
  60.4 0.0 all-gather.4.cloned.1.call-start
  60.5 0.5 all-gather.4.cloned.1.call-update
  61.0 0.0 all-gather.6.cloned.1.call-start
  61.1 0.5 all-gather.6.cloned.1.call-update
  61.6 0.0 all-gather.8.cloned.1.call-start
  61.7 0.5 all-gather.8.cloned.1.call-update
  62.2 0.0 all-reduce.5.cloned.1.call-start
  62.2 34.5 %all-reduce.3.cloned.1.call-done = bf16[128,2048]{1,0:T(8,128)(2,1)} async-done(((bf16[128,2048]{1,0:T(8,128)(2,1)}), bf16[128,2048]{1,0:T(8,128)(2,1)}) %all-reduce.3.cloned.1.call-update) | async-done | bytes 524304 | tf_op jit(solution)/shard_map/psum | solution.py:114
  96.8 1.2 fusion.12
  98.0 0.0 copy-done.1
  98.0 0.0 copy-done.2
  98.0 1.5 fusion.18
  99.5 63.6 %all-gather.4.cloned.1.call-done = bf16[2048,1280]{1,0:T(8,128)(2,1)} async-done(((bf16[512,1280]{1,0:T(8,128)(2,1)}), bf16[2048,1280]{1,0:T(8,128)(2,1)}) %all-gather.4.cloned.1.call-update) | async-done | bytes 5242896 | tf_op jit(solution)/shard_map/all_gather | solution.py:121
  163.1 3.4 fusion.30
  166.5 0.0 copy-start.4
  166.5 94.3 %all-gather.6.cloned.1.call-done = bf16[2048,1280]{1,0:T(8,128)(2,1)} async-done(((bf16[512,1280]{1,0:T(8,128)(2,1)}), bf16[2048,1280]{1,0:T(8,128)(2,1)}) %all-gather.6.cloned.1.call-update) | async-done | bytes 5242896 | tf_op jit(solution)/shard_map/all_gather | solution.py:126
  260.8 97.7 %all-gather.8.cloned.1.call-done = bf16[2048,1280]{1,0:T(8,128)(2,1)} async-done(((bf16[512,1280]{1,0:T(8,128)(2,1)}), bf16[2048,1280]{1,0:T(8,128)(2,1)}) %all-gather.8.cloned.1.call-update) | async-done | bytes 5242896 | tf_op jit(solution)/shard_map/all_gather | solution.py:132
  358.5 7.2 %convolution_convert_fusion = bf16[128,2048]{1,0:T(8,128)(2,1)} fusion(bf16[2048,1280]{1,0:T(8,128)(2,1)} %all-gather.8.cloned.1.call-done, bf16[2048,1280]{1,0:T(8,128)(2,1)} %all-gather.6.cloned.1.call-done, f32[128,1280]{1,0:T(8,128)S(1)} %fusion.30, bf16[128,2048]{1,0:T(8,128)(2,1)S(1)} %get-tuple-element.241, f32[128]{0:T(128)S(1)} %add_rsqrt_fusion.1, ...), kind=kOutput, calls=%fused_computation.23 | convolution fusion | flops 1344471040 | bytes 12198400 | tf_op jit(solution)/shard_map/dot_general | solution.py:130
  365.7 0.0 all-reduce.5.cloned.1.call-update
  365.7 31.9 %all-reduce.5.cloned.1.call-done = bf16[128,2048]{1,0:T(8,128)(2,1)} async-done(((bf16[128,2048]{1,0:T(8,128)(2,1)}), bf16[128,2048]{1,0:T(8,128)(2,1)}) %all-reduce.5.cloned.1.call-update) | async-done | bytes 524304 | tf_op jit(solution)/shard_map/psum | solution.py:136
  397.6 1.2 fusion.16
  398.9 2.1 fusion.21
  (26 shorter events, 0.3 us)
Async XLA Ops:
  7.4 51.9 %copy-start = (bf16[256,2048]{1,0:T(8,128)(2,1)S(1)}, bf16[256,2048]{1,0:T(8,128)(2,1)}, u32[]{:S(2)}) copy-start(bf16[256,2048]{1,0:T(8,128)(2,1)} %param.21) | copy-start | bytes 3145732
  7.4 89.4 %all-reduce.3.cloned.1.call-start = ((), (), s32[]{:S(2)}) async-start(), calls=%async_computation | async-start | bytes 1048576 | tf_op jit(solution)/shard_map/psum | solution.py:114
  57.2 40.8 %copy-start.1 = (bf16[128,2048]{1,0:T(8,128)(2,1)S(1)}, bf16[128,2048]{1,0:T(8,128)(2,1)}, u32[]{:S(2)}) copy-start(bf16[128,2048]{1,0:T(8,128)(2,1)} %param.20) | copy-start | bytes 1572868
  57.2 40.8 %copy-start.2 = (f32[2048]{0:T(1024)S(1)}, f32[2048]{0:T(1024)}, u32[]{:S(2)}) copy-start(f32[2048]{0:T(1024)} %param.22) | copy-start | bytes 24580
  57.2 105.8 %copy-start.3 = (f32[2048]{0:T(1024)S(1)}, f32[2048]{0:T(1024)}, u32[]{:S(2)}) copy-start(f32[2048]{0:T(1024)} %param.23) | copy-start | bytes 24580
  60.4 102.6 %all-gather.4.cloned.1.call-start = ((), (), s32[]{:S(2)}) async-start(), calls=%async_computation.1 | async-start | bytes 6553600 | tf_op jit(solution)/shard_map/all_gather | solution.py:121
  61.0 199.8 %all-gather.6.cloned.1.call-start = ((), (), s32[]{:S(2)}) async-start(), calls=%async_computation.2 | async-start | bytes 6553600 | tf_op jit(solution)/shard_map/all_gather | solution.py:126
  61.6 296.9 %all-gather.8.cloned.1.call-start = ((), (), s32[]{:S(2)}) async-start(), calls=%async_computation.3 | async-start | bytes 6553600 | tf_op jit(solution)/shard_map/all_gather | solution.py:132
  62.2 335.4 %all-reduce.5.cloned.1.call-start = ((), (), s32[]{:S(2)}) async-start(), calls=%async_computation.4 | async-start | bytes 1048576 | tf_op jit(solution)/shard_map/psum | solution.py:136
  166.5 232.4 %copy-start.4 = (f32[2048]{0:T(1024)S(1)}, f32[2048]{0:T(1024)}, u32[]{:S(2)}) copy-start(f32[2048]{0:T(1024)} %param.24) | copy-start | bytes 24580
Sparse Core Ops, SparseCore 0:
  60.6 36.1 all-reduce.2
  365.9 31.7 all-reduce.4
Sparse Core Ops, SparseCore 1:
  62.5 100.5 all-gather.3
  164.5 96.2 all-gather.5
  262.2 96.2 all-gather.7
where the time goes:
time: 409 us
  waiting for transfers between devices  324 us (79%)
  blocking collectives  39.1 us (10%)
  between operations  15.1 us (4%)
  matrix products  14 us (3%)
  other arithmetic  10.2 us (2%)
  local copies, waits for them, and re-layouts  4.28 us (1%)
    all_gather x1, waiting for transfers between devices, shards(): lax.all_gather(down_weight, 'sp', axis=0, tiled=True)  97.7 us
    all_gather x1, waiting for transfers between devices, shards(): lax.all_gather(up_weight, 'sp', axis=0, tiled=True)  94.3 us
    all_gather x1, waiting for transfers between devices, shards(): lax.all_gather(gate_weight, 'sp', axis=0, tiled=True)  63.6 us
    psum x1, waiting for transfers between devices, shards(): mixed_rows = lax.psum(head_part.astype(jnp.bfloat16), 'tp')  34.5 us
    psum x1, waiting for transfers between devices, shards(): ffn_out = lax.psum(unit_part.astype(jnp.bfloat16), 'tp')  31.9 us
    all_gather x1, blocking collectives, shards(): value_part = lax.all_gather(value_rows, 'sp', axis=0, tiled=True)  14.6 us
    all_gather x1, blocking collectives, shards(): key_part = lax.all_gather(key_rows, 'sp', axis=0, tiled=True)  14.5 us
    all_gather x1, blocking collectives, shards(): logit_part = lax.all_gather(key_logit, 'sp', axis=0, tiled=True)  10 us
  transfers between devices with their start and end apart: 5, of which 5 were waited for; matrix products, arithmetic and copies ran while one was open for 1% of the time, Pallas kernels for 0%

commit v1 on v0

--- a/solution.py
+++ b/solution.py
@@ -80,8 +80,11 @@
     )
     tables = initial
     key_part = lax.all_gather(key_rows, "sp", axis=0, tiled=True)
-    value_part = lax.all_gather(value_rows, "sp", axis=0, tiled=True)
-    logit_part = lax.all_gather(key_logit, "sp", axis=0, tiled=True)
+    value_part, logit_part = jnp.split(
+        lax.all_gather(jnp.concatenate([value_rows, key_logit], axis=1), "sp", axis=0, tiled=True),
+        [value_rows.shape[1]],
+        axis=1,
+    )
     shard_count = key_part.shape[0] // tok_rows
     group_size = 2
     span_rows = group_size * tok_rows

time: 409 us -> 405 us (level)
  blocking collectives: 39.1 us -> 29.6 us
    all_gather x2 -> x1, blocking collectives: 24.6 us -> 16.3 us  [shards(): lax.all_gather(jnp.concatenate([value_rows, key_logit], axis=1), 'sp', ax...]
  transfers between devices with their start and end apart: 5 -> 5, of which waited for: 5 -> 5; matrix products, arithmetic and copies ran while one was open for 1% -> 2% of each run, Pallas kernels for 0% -> 0%
where the time goes in v1:
time: 405 us; the launch traced here: 404 us
  waiting for transfers between devices  327 us (81%)
  blocking collectives  29.6 us (7%)
  between operations  15.2 us (4%)
  matrix products  14 us (3%)
  other arithmetic  11 us (3%)
  local copies, waits for them, and re-layouts  5.22 us (1%)
    all_gather x1, waiting for transfers between devices, shards(): lax.all_gather(down_weight, 'sp', axis=0, tiled=True)  97.7 us
    all_gather x1, waiting for transfers between devices, shards(): lax.all_gather(up_weight, 'sp', axis=0, tiled=True)  94.3 us
    all_gather x1, waiting for transfers between devices, shards(): lax.all_gather(gate_weight, 'sp', axis=0, tiled=True)  63.6 us
    psum x1, waiting for transfers between devices, shards(): mixed_rows = lax.psum(head_part.astype(jnp.bfloat16), 'tp')  37.6 us
    psum x1, waiting for transfers between devices, shards(): ffn_out = lax.psum(unit_part.astype(jnp.bfloat16), 'tp')  31.9 us
    all_gather x1, blocking collectives, shards(): lax.all_gather(jnp.concatenate([value_rows, key_logit], axis=1), 'sp', ax...  16.3 us
    all_gather x1, blocking collectives, shards(): key_part = lax.all_gather(key_rows, 'sp', axis=0, tiled=True)  13.4 us
  transfers between devices with their start and end apart: 5, of which 5 were waited for; matrix products, arithmetic and copies ran while one was open for 2% of the time, Pallas kernels for 0%

profile of v1, /device:TPU:0, one launch (start us, length us, event | category | flops | bytes accessed | tf_op | source)
XLA Modules:
  0.0 404.0 jit_solution(16098828212318033610)
XLA Ops:
  7.4 0.9 copy.47
  8.2 0.9 pad_maximum_fusion
  9.1 16.3 %all_gather.16 = bf16[512,258]{1,0:T(8,128)(2,1)S(1)} all-gather(bf16[128,258]{1,0:T(8,128)(2,1)S(1)} %pad_maximum_fusion), channel_id=1, replica_groups=mesh['grp'=2,'sp'=4,'tp'=4] {'sp'}, dimensions={0}, use_global_device_ids=true | all-gather | bytes 330240 | tf_op jit(solution)/shard_map/all_gather | solution.py:84
  25.4 0.1 copy.49
  25.5 1.0 copy.45
  26.5 13.4 %all_gather.15 = bf16[512,256]{0,1:T(8,128)(2,1)S(1)} all-gather(bf16[128,256]{0,1:T(8,128)(2,1)S(1)} %copy.45), channel_id=1, replica_groups=mesh['grp'=2,'sp'=4,'tp'=4] {'sp'}, dimensions={0}, use_global_device_ids=true | all-gather | bytes 327680 | tf_op jit(solution)/shard_map/all_gather | solution.py:82
  39.9 0.9 copy.46
  40.8 0.1 copy.48
  41.0 0.1 broadcast_in_dim.28.clone
  41.0 8.5 %while.13 = (s32[]{:T(128)}, f32[2,128,4]{1,2,0:T(4,128)S(1)}, f32[4,2,128,128]{3,0,1,2:T(4,128)S(1)}, s32[2]{0:T(128)S(1)}, s32[]{:T(128)}, /*index=5*/bf16[512...) while((s32[]{:T(128)}, f32[2,128,4]{1,2,0:T(4,128)S(1)}, ...), condition=%wide.region_5.6_spmd.clone, body=%wide.region_0.5_spmd.clone.sunk | while | flops 43418504 | bytes 4373875 | solution.py:107
  41.1 0.6 dynamic_slice.39
  42.3 5.3 %conditional.3 = (f32[2,128,2]{1,2,0:T(2,128)S(1)}, f32[2,2,128,128]{3,2,1,0:T(8,128)S(1)}) conditional(s32[]{:T(128)} %convert_element_type.116, () %tuple.49, (s32[]{:T(128)}, s32[]{:T(128)}, s32[]{:T(128)}, bf16[512,256]{0,1:T(8,128)(2,1)S(1)}, bf16[2,128,128]{2,1,0:T(8,128)(2,1)S(1)}, /*index=5*/bf16[512,2]{0,1:T(2,128)(2,1)S(1)}, ...), branch_computations={%region_1.1_spmd, %region_2.4_spmd} | conditional | flops 43418500 | bytes 3844702 | solution.py:75
  43.0 0.2 fusion.2
  43.3 0.2 broadcast_compare_fusion
  43.5 0.8 fusion.35
  44.2 2.2 fusion.38
  46.4 0.9 select_convert_fusion
  47.4 0.2 fusion.8
  47.6 0.3 copy_dynamic-update-slice_fusion.2
  48.0 0.6 dynamic_slice.39
  49.3 0.3 copy_dynamic-update-slice_fusion.2
  49.6 0.0 copy-start.1
  49.6 0.0 copy-start.2
  49.6 0.0 copy-start.3
  49.7 0.2 copy.51
  49.8 1.8 fusion.39
  51.7 1.1 convolution_convert_fusion.1
  52.8 0.0 all-reduce.3.cloned.1.call-update
  52.9 0.0 all-gather.4.cloned.1.call-start
  52.9 0.5 all-gather.4.cloned.1.call-update
  53.4 0.0 all-gather.6.cloned.1.call-start
  53.5 0.5 all-gather.6.cloned.1.call-update
  54.0 0.0 all-gather.8.cloned.1.call-start
  54.1 0.5 all-gather.8.cloned.1.call-update
  54.6 0.0 all-reduce.5.cloned.1.call-start
  54.6 37.6 %all-reduce.3.cloned.1.call-done = bf16[128,2048]{1,0:T(8,128)(2,1)} async-done(((bf16[128,2048]{1,0:T(8,128)(2,1)}), bf16[128,2048]{1,0:T(8,128)(2,1)}) %all-reduce.3.cloned.1.call-update) | async-done | bytes 524304 | tf_op jit(solution)/shard_map/psum | solution.py:117
  92.3 1.2 fusion.12
  93.5 1.5 fusion.18
  95.0 63.6 %all-gather.4.cloned.1.call-done = bf16[2048,1280]{1,0:T(8,128)(2,1)} async-done(((bf16[512,1280]{1,0:T(8,128)(2,1)}), bf16[2048,1280]{1,0:T(8,128)(2,1)}) %all-gather.4.cloned.1.call-update) | async-done | bytes 5242896 | tf_op jit(solution)/shard_map/all_gather | solution.py:124
  158.6 3.4 fusion.30
  162.0 0.0 copy-start.4
  162.0 94.3 %all-gather.6.cloned.1.call-done = bf16[2048,1280]{1,0:T(8,128)(2,1)} async-done(((bf16[512,1280]{1,0:T(8,128)(2,1)}), bf16[2048,1280]{1,0:T(8,128)(2,1)}) %all-gather.6.cloned.1.call-update) | async-done | bytes 5242896 | tf_op jit(solution)/shard_map/all_gather | solution.py:129
  256.3 97.7 %all-gather.8.cloned.1.call-done = bf16[2048,1280]{1,0:T(8,128)(2,1)} async-done(((bf16[512,1280]{1,0:T(8,128)(2,1)}), bf16[2048,1280]{1,0:T(8,128)(2,1)}) %all-gather.8.cloned.1.call-update) | async-done | bytes 5242896 | tf_op jit(solution)/shard_map/all_gather | solution.py:135
  354.0 7.2 %convolution_convert_fusion = bf16[128,2048]{1,0:T(8,128)(2,1)} fusion(bf16[2048,1280]{1,0:T(8,128)(2,1)} %all-gather.8.cloned.1.call-done, bf16[2048,1280]{1,0:T(8,128)(2,1)} %all-gather.6.cloned.1.call-done, f32[128,1280]{1,0:T(8,128)S(1)} %fusion.30, bf16[128,2048]{1,0:T(8,128)(2,1)S(1)} %get-tuple-element.251, f32[128]{0:T(128)S(1)} %add_rsqrt_fusion.1, ...), kind=kOutput, calls=%fused_computation.23 | convolution fusion | flops 1344471040 | bytes 12198400 | tf_op jit(solution)/shard_map/dot_general | solution.py:133
  361.2 0.0 all-reduce.5.cloned.1.call-update
  361.2 31.9 %all-reduce.5.cloned.1.call-done = bf16[128,2048]{1,0:T(8,128)(2,1)} async-done(((bf16[128,2048]{1,0:T(8,128)(2,1)}), bf16[128,2048]{1,0:T(8,128)(2,1)}) %all-reduce.5.cloned.1.call-update) | async-done | bytes 524304 | tf_op jit(solution)/shard_map/psum | solution.py:139
  393.1 1.2 fusion.16
  394.4 2.1 fusion.21
  (30 shorter events, 0.4 us)
Async XLA Ops:
  7.4 44.3 %copy-start = (bf16[256,2048]{1,0:T(8,128)(2,1)S(1)}, bf16[256,2048]{1,0:T(8,128)(2,1)}, u32[]{:S(2)}) copy-start(bf16[256,2048]{1,0:T(8,128)(2,1)} %param.21) | copy-start | bytes 3145732
  7.4 84.9 %all-reduce.3.cloned.1.call-start = ((), (), s32[]{:S(2)}) async-start(), calls=%async_computation | async-start | bytes 1048576 | tf_op jit(solution)/shard_map/psum | solution.py:117
  49.6 43.9 %copy-start.1 = (bf16[128,2048]{1,0:T(8,128)(2,1)S(1)}, bf16[128,2048]{1,0:T(8,128)(2,1)}, u32[]{:S(2)}) copy-start(bf16[128,2048]{1,0:T(8,128)(2,1)} %param.20) | copy-start | bytes 1572868
  49.6 43.9 %copy-start.2 = (f32[2048]{0:T(1024)S(1)}, f32[2048]{0:T(1024)}, u32[]{:S(2)}) copy-start(f32[2048]{0:T(1024)} %param.22) | copy-start | bytes 24580
  49.6 109.0 %copy-start.3 = (f32[2048]{0:T(1024)S(1)}, f32[2048]{0:T(1024)}, u32[]{:S(2)}) copy-start(f32[2048]{0:T(1024)} %param.23) | copy-start | bytes 24580
  52.9 105.7 %all-gather.4.cloned.1.call-start = ((), (), s32[]{:S(2)}) async-start(), calls=%async_computation.1 | async-start | bytes 6553600 | tf_op jit(solution)/shard_map/all_gather | solution.py:124
  53.4 202.8 %all-gather.6.cloned.1.call-start = ((), (), s32[]{:S(2)}) async-start(), calls=%async_computation.2 | async-start | bytes 6553600 | tf_op jit(solution)/shard_map/all_gather | solution.py:129
  54.0 300.0 %all-gather.8.cloned.1.call-start = ((), (), s32[]{:S(2)}) async-start(), calls=%async_computation.3 | async-start | bytes 6553600 | tf_op jit(solution)/shard_map/all_gather | solution.py:135
  54.6 338.5 %all-reduce.5.cloned.1.call-start = ((), (), s32[]{:S(2)}) async-start(), calls=%async_computation.4 | async-start | bytes 1048576 | tf_op jit(solution)/shard_map/psum | solution.py:139
  162.0 232.4 %copy-start.4 = (f32[2048]{0:T(1024)S(1)}, f32[2048]{0:T(1024)}, u32[]{:S(2)}) copy-start(f32[2048]{0:T(1024)} %param.24) | copy-start | bytes 24580
Sparse Core Ops, SparseCore 0:
  53.0 39.2 all-reduce.2
  361.4 31.7 all-reduce.4
Sparse Core Ops, SparseCore 1:
  54.9 103.6 all-gather.3
  160.0 96.2 all-gather.5
  257.7 96.2 all-gather.7
